TPU v7x, 32 devices: a whole 2x2x4 slice. The times are simulated.
32 devices in a mesh: sp: 8 (over z, x), tp: 4 (over y, core).
Axes of the slice: x: 2, y: 2, z: 4, core: 2. Of those that a mesh axis runs over, the one named last changes fastest.
Arguments:
- queries: bfloat16 [8192, 1536], P('sp', 'tp'), may hold values from -200 to 200
- key_heads: bfloat16 [8192, 512], P('sp', 'tp'), may hold values from -6 to 6
- projected_value_heads: bfloat16 [8192, 512], P('sp', 'tp'), may hold values from -5 to 5
- sink_logit_table: float32 [24], P('tp'), may hold values from 0 to 4
- out_weight: bfloat16 [1536, 3072], P('tp'), may hold values from -1.5 to 1.5
- residual: bfloat16 [8192, 3072], P('sp', 'tp'), may hold values from -16 to 16
- norm_gain: bfloat16 [3072], P('tp'), may hold values from 0.099609375 to 1.8984375
- up_weight: bfloat16 [3072, 12288], P('sp', 'tp'), may hold values from -0.109375 to 0.109375
- down_weight: bfloat16 [12288, 3072], P('tp', 'sp'), may hold values from -0.0546875 to 0.0546875
Outputs:
- result: bfloat16 [8192, 3072], P('sp', 'tp')
All inputs are finite; a program needn't handle non-finite values.
Results may differ from a plain program's by a relative error of at most 0.015.
Values may be sent and summed in bfloat16 or wider, within the bound.
No kernel may reach another device: no remote copies, remote signals or barrier semaphores. Data moves between devices by JAX's collectives and lax.ppermute only.
A program may use at most 128 MiB of HBM per device.

v0:
```python
import jax
import jax.numpy as jnp
from jax import lax
from jax.sharding import PartitionSpec as P

D = 3072
HEAD_SIZE = 64
WINDOW_SPAN = 128


epsilon = 1e-06


def shifted(block, axis, distance):
    devices = range(lax.axis_size(axis))
    route = [(i - distance, i) for i in devices if i - distance in devices]
    return lax.ppermute(block, axis, route)


def attend(queries, key_heads, projected_value_heads, sink_logit_table, previous, offset):
    row_count = queries.shape[0]
    kv_cols = key_heads.shape[1]
    kv_local = kv_cols // HEAD_SIZE
    group_count = queries.shape[1] // kv_cols
    block_count = row_count // WINDOW_SPAN
    extended_keys = jnp.concatenate([previous[:, :kv_cols], key_heads], axis=0)
    extended_values = jnp.concatenate([previous[:, kv_cols:], projected_value_heads], axis=0)

    def banded(source_rows):
        shaped = source_rows.reshape(block_count + 1, WINDOW_SPAN, kv_local, HEAD_SIZE)
        return jnp.concatenate([shaped[:-1], shaped[1:]], axis=1)

    key_band = banded(extended_keys)
    value_band = banded(extended_values)
    query_block_list = queries.reshape(block_count, WINDOW_SPAN, kv_local, group_count, HEAD_SIZE)
    scores = jnp.einsum(
        "nqkgd,nskd->nkgqs", query_block_list, key_band, preferred_element_type=jnp.float32
    ) * HEAD_SIZE ** (-0.5)
    within = jnp.arange(WINDOW_SPAN)[:, None]
    column = jnp.arange(2 * WINDOW_SPAN)[None, :]
    distance = WINDOW_SPAN + within - column
    valid = (distance >= 0) & (distance < WINDOW_SPAN)
    key_pos = (
        offset
        + jnp.arange(block_count)[:, None] * WINDOW_SPAN
        + jnp.arange(2 * WINDOW_SPAN)[None, :]
        - WINDOW_SPAN
    )
    allowed = valid[None] & (key_pos >= 0)[:, None, :]
    allowed = allowed[:, None, None]
    head_sink_logit = sink_logit_table.reshape(kv_local, group_count)[None, :, :, None, None]
    masked = jnp.where(allowed, scores, -1e30)
    ceiling = jnp.maximum(jnp.max(masked, axis=-1, keepdims=True), head_sink_logit)
    powers = jnp.where(allowed, jnp.exp(masked - ceiling), 0.0)
    denom = jnp.sum(powers, axis=-1, keepdims=True) + jnp.exp(head_sink_logit - ceiling)
    probs = (powers / denom).astype(jnp.bfloat16)
    output = jnp.einsum("nkgqs,nskd->nqkgd", probs, value_band, preferred_element_type=jnp.float32)
    return output.astype(jnp.bfloat16).reshape(row_count, queries.shape[1])


def rounded(values):
    return lax.optimization_barrier(values.astype(jnp.bfloat16)).astype(jnp.float32)


def body(
    queries,
    key_heads,
    projected_value_heads,
    sink_logit_table,
    out_weight,
    residual,
    norm_gain,
    up_weight,
    down_weight,
):
    row_count = queries.shape[0]
    offset = lax.axis_index("sp") * row_count
    tail = jnp.concatenate(
        [key_heads[row_count - WINDOW_SPAN :], projected_value_heads[row_count - WINDOW_SPAN :]],
        axis=1,
    )
    previous = shifted(tail, "sp", 1)
    attended = attend(queries, key_heads, projected_value_heads, sink_logit_table, previous, offset)
    partial_value = rounded(jnp.dot(attended, out_weight, preferred_element_type=jnp.float32))
    mixed_sum = lax.psum_scatter(
        partial_value.astype(jnp.bfloat16), "tp", scatter_dimension=1, tiled=True
    ).astype(jnp.float32)
    stream = rounded(residual.astype(jnp.float32) + mixed_sum)
    squares = lax.psum(jnp.sum(stream * stream, axis=1, keepdims=True), "tp")
    normed = (stream * lax.rsqrt(squares / D + epsilon) * norm_gain.astype(jnp.float32)).astype(
        jnp.bfloat16
    )
    normed_whole = lax.all_gather(normed, "tp", axis=1, tiled=True)
    hidden_pre = jnp.dot(
        normed_whole,
        lax.all_gather(up_weight, "sp", axis=0, tiled=True),
        preferred_element_type=jnp.float32,
    )
    activated = jnp.square(jax.nn.relu(hidden_pre)).astype(jnp.bfloat16)
    terms = jnp.dot(
        activated,
        lax.all_gather(down_weight, "sp", axis=1, tiled=True),
        preferred_element_type=jnp.float32,
    )
    branch_sum = lax.psum_scatter(
        rounded(terms).astype(jnp.bfloat16), "tp", scatter_dimension=1, tiled=True
    ).astype(jnp.float32)
    return (stream + branch_sum).astype(jnp.bfloat16)


def solution(mesh):
    return jax.shard_map(
        body,
        mesh=mesh,
        in_specs=(
            P("sp", "tp"),
            P("sp", "tp"),
            P("sp", "tp"),
            P("tp"),
            P("tp", None),
            P("sp", "tp"),
            P("tp"),
            P("sp", "tp"),
            P("tp", "sp"),
        ),
        out_specs=P("sp", "tp"),
        check_vma=False,
    )
```

profile of v0, /device:TPU:0, one launch (start us, length us, event | category | flops | bytes accessed | tf_op | source)
XLA Modules:
  0.0 985.8 jit_solution(6724844009850247608)
XLA Ops:
  6.5 0.9 slice.32
  7.5 0.8 slice.33
  8.2 4.9 collective-permute-start
  13.2 0.1 add_compare_fusion
  13.3 1.0 broadcast_and_fusion
  14.3 2.0 reshape.91
  16.3 2.0 reshape.89
  18.3 1.4 copy.20
  19.7 1.1 copy.35
  20.8 1.9 copy.19
  22.7 0.7 max.26
  23.4 1.9 copy.15
  25.3 1.7 pad_maximum_fusion
  27.0 1.2 reshape.90
  28.2 1.0 copy.18
  29.2 2.5 fusion
  31.7 0.1 broadcast_maximum_fusion
  31.7 2.6 copy-done.3
  34.3 2.8 fusion.1
  37.1 0.1 exponential_add_fusion
  37.2 0.2 reshape.88
  37.5 0.4 copy.14
  37.9 4.9 fusion.8
  42.7 0.5 copy.23
  43.3 0.0 copy-start.6
  43.3 5.4 convolution_convert_fusion.1
  48.7 0.0 reduce-scatter.3.cloned.1.call-update
  48.7 0.0 all-gather.4.cloned.1.call-start
  48.8 58.3 %reduce-scatter.3.cloned.1.call-done = bf16[1024,768]{1,0:T(8,128)(2,1)} async-done(((bf16[1024,3072]{1,0:T(8,128)(2,1)}), bf16[1024,768]{1,0:T(8,128)(2,1)}) %reduce-scatter.3.cloned.1.call-update) | async-done | bytes 1572880 | tf_op jit(solution)/shard_map/reduce_scatter | solution.py:85
  107.1 2.3 add_convert_fusion
  109.3 0.0 copy-start.2
  109.3 0.4 fusion.2
  109.7 5.8 psum.7
  115.5 1.5 fusion.4
  117.0 0.0 all-gather.4.cloned.1.call-update
  117.1 0.0 all-gather.6.cloned.1.call-start
  117.1 0.7 all-gather.6.cloned.1.call-update
  117.8 0.0 all-gather.8.cloned.1.call-start
  117.9 0.5 all-gather.8.cloned.1.call-update
  118.4 0.2 reduce-scatter.5.cloned.1.call-start
  118.6 45.6 %all-gather.4.cloned.1.call-done = bf16[1024,3072]{1,0:T(8,128)(2,1)} async-done(((bf16[1024,768]{1,0:T(8,128)(2,1)}), bf16[1024,3072]{1,0:T(8,128)(2,1)}) %all-gather.4.cloned.1.call-update) | async-done | bytes 6291472 | tf_op jit(solution)/shard_map/all_gather | solution.py:93
  164.2 364.0 %all-gather.6.cloned.1.call-done = bf16[3072,3072]{1,0:T(8,128)(2,1)} async-done(((bf16[384,3072]{1,0:T(8,128)(2,1)}), bf16[3072,3072]{1,0:T(8,128)(2,1)}) %all-gather.6.cloned.1.call-update) | async-done | bytes 18874384 | tf_op jit(solution)/shard_map/all_gather | solution.py:96
  528.2 25.8 %multiply_convert_fusion.clone.4 = bf16[1024,3072]{1,0:T(8,128)(2,1)} fusion(bf16[1024,3072]{1,0:T(8,128)(2,1)} %all-gather.4.cloned.1.call-done, bf16[3072,3072]{1,0:T(8,128)(2,1)} %all-gather.6.cloned.1.call-done), kind=kOutput, calls=%fused_computation.clone.clone.clone.1 | convolution fusion | flops 19336790016 | bytes 31457280 | tf_op jit(solution)/shard_map/dot_general | solution.py:94
  553.9 338.0 %all-gather.8.cloned.1.call-done = bf16[3072,3072]{1,0:T(8,128)(2,1)} async-done(((bf16[3072,384]{1,0:T(8,128)(2,1)}), bf16[3072,3072]{1,0:T(8,128)(2,1)}) %all-gather.8.cloned.1.call-update) | async-done | bytes 18874384 | tf_op jit(solution)/shard_map/all_gather | solution.py:102
  892.0 25.8 %convolution_convert_fusion = bf16[1024,3072]{1,0:T(8,128)(2,1)} fusion(bf16[3072,3072]{1,0:T(8,128)(2,1)} %all-gather.8.cloned.1.call-done, bf16[1024,3072]{1,0:T(8,128)(2,1)} %multiply_convert_fusion.clone.4), kind=kOutput, calls=%fused_computation.4 | convolution fusion | flops 19330498560 | bytes 31457280 | tf_op jit(solution)/shard_map/dot_general | solution.py:100
  917.8 0.0 reduce-scatter.5.cloned.1.call-update
  917.9 58.0 %reduce-scatter.5.cloned.1.call-done = bf16[1024,768]{1,0:T(8,128)(2,1)} async-done(((bf16[1024,3072]{1,0:T(8,128)(2,1)}), bf16[1024,768]{1,0:T(8,128)(2,1)}) %reduce-scatter.5.cloned.1.call-update) | async-done | bytes 1572880 | tf_op jit(solution)/shard_map/reduce_scatter | solution.py:105
  975.9 3.4 fusion.5
  (20 shorter events, 0.1 us)
Async XLA Ops:
  6.5 36.7 %copy-start = (bf16[384,3072]{1,0:T(8,128)(2,1)S(1)}, bf16[384,3072]{1,0:T(8,128)(2,1)}, u32[]{:S(2)}) copy-start(bf16[384,3072]{1,0:T(8,128)(2,1)} %param.13) | copy-start | bytes 7077892
  6.5 18.8 %copy-start.4 = (bf16[1024,128]{1,0:T(8,128)(2,1)S(1)}, bf16[1024,128]{1,0:T(8,128)(2,1)}, u32[]{:S(2)}) copy-start(bf16[1024,128]{1,0:T(8,128)(2,1)} %param.10) | copy-start | bytes 786436
  6.5 100.5 %reduce-scatter.3.cloned.1.call-start = ((), (), s32[]{:S(2)}) async-start(), calls=%async_computation.2 | async-start | bytes 7864320 | tf_op jit(solution)/shard_map/reduce_scatter | solution.py:85
  8.2 17.1 %collective-permute-start = (bf16[128,256]{1,0:T(8,128)(2,1)S(1)}, bf16[128,256]{1,0:T(8,128)(2,1)S(1)}, u32[]{:S(2)}, u32[]{:S(2)}) collective-permute-start(bf16[128,256]{1,0:T(8,128)(2,1)S(1)} %pad_maximum_fusion.2), channel_id=1, source_target_pairs={{0,4},{4,8},{8,12},{12,16},{16,20},{20,24},{24,28},{1,5},{5,9},{9,... | collective-permute-start | bytes 196616 | tf_op jit(solution)/shard_map/ppermute | solution.py:17
  29.1 8.7 copy-start.5
  31.6 2.7 copy-start.3
  43.3 5.5 copy-start.6
  48.7 115.5 %all-gather.4.cloned.1.call-start = ((), (), s32[]{:S(2)}) async-start(), calls=%async_computation.3 | async-start | bytes 7864320 | tf_op jit(solution)/shard_map/all_gather | solution.py:93
  109.3 444.6 %copy-start.2 = (bf16[1024,768]{1,0:T(8,128)(2,1)}, bf16[1024,768]{1,0:T(8,128)(2,1)S(1)}, u32[]{:S(2)}) copy-start(bf16[1024,768]{1,0:T(8,128)(2,1)S(1)} %add_convert_fusion) | copy-start | bytes 4718596
  117.1 411.1 %all-gather.6.cloned.1.call-start = ((), (), s32[]{:S(2)}) async-start(), calls=%async_computation.4 | async-start | bytes 21233664 | tf_op jit(solution)/shard_map/all_gather | solution.py:96
  117.8 774.2 %all-gather.8.cloned.1.call-start = ((), (), s32[]{:S(2)}) async-start(), calls=%async_computation.5 | async-start | bytes 21233664 | tf_op jit(solution)/shard_map/all_gather | solution.py:102
  118.4 857.5 %reduce-scatter.5.cloned.1.call-start = ((), (), s32[]{:S(2)}) async-start(), calls=%async_computation.6 | async-start | bytes 7864320 | tf_op jit(solution)/shard_map/reduce_scatter | solution.py:105
  892.0 87.3 %copy-start.1 = (bf16[384,3072]{1,0:T(8,128)(2,1)S(1)}, bf16[384,3072]{1,0:T(8,128)(2,1)}, u32[]{:S(2)}) copy-start(bf16[384,3072]{1,0:T(8,128)(2,1)} %param.13) | copy-start | bytes 7077892
Sparse Core Ops, SparseCore 0:
  48.8 58.1 reduce-scatter.2
  117.2 46.9 all-gather.3
  165.8 362.3 all-gather.5
  529.6 362.3 all-gather.7
  918.0 57.8 reduce-scatter.4
where the time goes:
time: 986 us
  waiting for transfers between devices  865 us (88%)
  matrix products  64.4 us (7%)
  local copies, waits for them, and re-layouts  18.5 us (2%)
  other arithmetic  13.4 us (1%)
  between operations  13.3 us (1%)
    all_gather x1, waiting for transfers between devices, body(): lax.all_gather(up_weight, 'sp', axis=0, tiled=True)  364 us
    all_gather x1, waiting for transfers between devices, body(): lax.all_gather(down_weight, 'sp', axis=1, tiled=True)  338 us
    reduce_scatter x1, waiting for transfers between devices, body(): lax.psum_scatter(partial_value.astype(jnp.bfloat16), 'tp', scatter_dimens...  58.3 us
    reduce_scatter x1, waiting for transfers between devices, body(): lax.psum_scatter(rounded(terms).astype(jnp.bfloat16), 'tp', scatter_dimen...  58 us
    all_gather x1, waiting for transfers between devices, body(): normed_whole = lax.all_gather(normed, 'tp', axis=1, tiled=True)  45.6 us
    dot_general x1, matrix products, body(): jnp.dot(activated, lax.all_gather(down_weight, 'sp', axis=1, tiled=True),...  25.8 us
    dot_general x1, matrix products, body(): jnp.dot(normed_whole, lax.all_gather(up_weight, 'sp', axis=0, tiled=True)...  25.8 us
  transfers between devices with their start and end apart: 6, of which 5 were waited for; matrix products, arithmetic and copies ran while one was open for 4% of the time, Pallas kernels for 0%

commit v1 on v0

--- a/solution.py
+++ b/solution.py
@@ -2,6 +2,7 @@
 import jax.numpy as jnp
 from jax import lax
 from jax.sharding import PartitionSpec as P
+
 
 D = 3072
 HEAD_SIZE = 64
@@ -35,7 +36,8 @@
     query_block_list = queries.reshape(block_count, WINDOW_SPAN, kv_local, group_count, HEAD_SIZE)
     scores = jnp.einsum(
         "nqkgd,nskd->nkgqs", query_block_list, key_band, preferred_element_type=jnp.float32
-    ) * HEAD_SIZE ** (-0.5)
+    )
+    scores = scores * HEAD_SIZE ** (-0.5)
     within = jnp.arange(WINDOW_SPAN)[:, None]
     column = jnp.arange(2 * WINDOW_SPAN)[None, :]
     distance = WINDOW_SPAN + within - column
@@ -58,6 +60,42 @@
     return output.astype(jnp.bfloat16).reshape(row_count, queries.shape[1])
 
 
+def loop_order(size):
+    return list(range(0, size, 2)) + list(range(size - 1, 0, -2))
+
+
+def walked(shard):
+    size = lax.axis_size("sp")
+    order = loop_order(size)
+    ahead = [(order[i], order[(i + 1) % size]) for i in range(size)]
+    behind = [(b, a) for a, b in ahead]
+
+    def send(block, route):
+        return lax.ppermute(block, "sp", route)
+
+    middle = shard.shape[0] // 2
+    above = below = shard
+    blocks = []
+    for step in range(1, size // 2):
+        above, below = send(above, ahead), send(below, behind)
+        blocks += [(-step, above), (step, below)]
+    far = (send(above[:middle], ahead), send(below[middle:], behind))
+    return blocks, far
+
+
+def place():
+    size = lax.axis_size("sp")
+    index = lax.axis_index("sp")
+    return jnp.where(index % 2 == 0, index // 2, size - 1 - index // 2)
+
+
+def source(step):
+    size = lax.axis_size("sp")
+    spot = (place() + step) % size
+    side = (spot >= size // 2).astype(jnp.int32)
+    return jnp.where(side == 0, spot, size - 1 - spot), side
+
+
 def rounded(values):
     return lax.optimization_barrier(values.astype(jnp.bfloat16)).astype(jnp.float32)
 
@@ -75,36 +113,56 @@
 ):
     row_count = queries.shape[0]
     offset = lax.axis_index("sp") * row_count
+    up_blocks, up_far = walked(up_weight)
+    down_blocks, down_far = walked(down_weight)
     tail = jnp.concatenate(
         [key_heads[row_count - WINDOW_SPAN :], projected_value_heads[row_count - WINDOW_SPAN :]],
         axis=1,
     )
     previous = shifted(tail, "sp", 1)
     attended = attend(queries, key_heads, projected_value_heads, sink_logit_table, previous, offset)
-    partial_value = rounded(jnp.dot(attended, out_weight, preferred_element_type=jnp.float32))
+    partial_value = jnp.dot(attended, out_weight, preferred_element_type=jnp.float32)
     mixed_sum = lax.psum_scatter(
         partial_value.astype(jnp.bfloat16), "tp", scatter_dimension=1, tiled=True
-    ).astype(jnp.float32)
+    )
+    mixed_sum = mixed_sum.astype(jnp.float32)
     stream = rounded(residual.astype(jnp.float32) + mixed_sum)
     squares = lax.psum(jnp.sum(stream * stream, axis=1, keepdims=True), "tp")
     normed = (stream * lax.rsqrt(squares / D + epsilon) * norm_gain.astype(jnp.float32)).astype(
         jnp.bfloat16
     )
     normed_whole = lax.all_gather(normed, "tp", axis=1, tiled=True)
-    hidden_pre = jnp.dot(
-        normed_whole,
-        lax.all_gather(up_weight, "sp", axis=0, tiled=True),
-        preferred_element_type=jnp.float32,
+    size = lax.axis_size("sp")
+    column = lax.axis_index("sp") % 2
+    rows = size // 2
+    deep = up_weight.shape[0]
+    wide = down_weight.shape[1]
+    up_whole = jnp.zeros((size * deep, up_weight.shape[1]), up_weight.dtype)
+    pieces = [(0, 0, up_weight)] + [(step, 0, block) for step, block in up_blocks]
+    pieces += [(rows, 0, up_far[0]), (rows, deep // 2, up_far[1])]
+    for step, top, block in pieces:
+        row, side = source(step)
+        start = (2 * row + side) * deep + top
+        up_whole = lax.dynamic_update_slice(up_whole, block, (start, 0))
+    hidden_pre = jnp.dot(normed_whole, up_whole, preferred_element_type=jnp.float32)
+    activated = jnp.square(jax.nn.relu(hidden_pre)).astype(jnp.bfloat16)
+
+    terms = jnp.zeros((size, row_count, wide), jnp.bfloat16)
+    for step, block in [(0, down_weight)] + down_blocks:
+        row, side = source(step)
+        term = jnp.dot(activated, block, preferred_element_type=jnp.float32)
+        at = jnp.where(side == column, row, rows + row)
+        terms = lax.dynamic_update_slice(terms, term.astype(jnp.bfloat16)[None], (at, 0, 0))
+    ours = lax.psum_scatter(terms[:rows], "tp", scatter_dimension=0, tiled=True)
+    term = jnp.dot(activated, jnp.concatenate(down_far, axis=0), preferred_element_type=jnp.float32)
+    second = lax.dynamic_update_slice(
+        terms[rows:], term.astype(jnp.bfloat16)[None], (source(rows)[0], 0, 0)
     )
-    activated = jnp.square(jax.nn.relu(hidden_pre)).astype(jnp.bfloat16)
-    terms = jnp.dot(
-        activated,
-        lax.all_gather(down_weight, "sp", axis=1, tiled=True),
-        preferred_element_type=jnp.float32,
-    )
-    branch_sum = lax.psum_scatter(
-        rounded(terms).astype(jnp.bfloat16), "tp", scatter_dimension=1, tiled=True
-    ).astype(jnp.float32)
+    theirs = lax.psum_scatter(second, "tp", scatter_dimension=0, tiled=True)
+    low = jnp.where(column == 0, ours, theirs)
+    high = jnp.where(column == 0, theirs, ours)
+    branch_sum = jnp.stack([low, high], axis=1).reshape(-1, row_count, wide)
+    branch_sum = branch_sum.transpose(1, 0, 2).reshape(row_count, -1).astype(jnp.float32)
     return (stream + branch_sum).astype(jnp.bfloat16)
 
 

time: 986 us -> 620 us (0.63)
  waiting for transfers between devices: 865 us -> 419 us
  local copies, waits for them, and re-layouts: 18.5 us -> 60 us
  starting transfers between devices: 5.22 us -> 21.9 us
  matrix products: 64.4 us -> 76.6 us
    all_gather x2 -> x0, waiting for transfers between devices: 702 us -> none  [the longest x1 364 us: body(): lax.all_gather(up_weight, 'sp', axis=0, tiled=True)]
    ppermute x0 -> x16, waiting for transfers between devices: none -> 282 us  [send(): return lax.ppermute(block, 'sp', route)]
    all_gather x1, waiting for transfers between devices: 45.6 us -> 0.01 us  [body(): normed_whole = lax.all_gather(normed, 'tp', axis=1, tiled=True)]
    dynamic_update_slice x0 -> x9, local copies, waits for them, and re-layouts: none -> 19.9 us  [body(): up_whole = lax.dynamic_update_slice(up_whole, block, (start, 0))]
    reduce_scatter x1 -> x2, waiting for transfers between devices: 58 us -> 77.9 us  [the longest x1 40.3 us: body(): ours = lax.psum_scatter(terms[:rows], 'tp', scatter_dimension=0, tiled=True)]
    ppermute x0 -> x16, starting transfers between devices: none -> 16.9 us  [send(): return lax.ppermute(block, 'sp', route)]
    slice x0 -> x5, local copies, waits for them, and re-layouts: none -> 9.91 us  [the longest x4 7.57 us: walked(): far = (send(above[:middle], ahead), send(below[middle:], behind))]
    dot_general x2 -> x9, matrix products: 51.6 us -> 61.1 us  [the longest x7 31.4 us: body(): term = jnp.dot(activated, block, preferred_element_type=jnp.float32)]
  transfers between devices with their start and end apart: 6 -> 21, of which waited for: 5 -> 11; matrix products, arithmetic and copies ran while one was open for 4% -> 17% of each run, Pallas kernels for 0% -> 0%
where the time goes in v1:
time: 620 us; the launch traced here: 611 us
  waiting for transfers between devices  419 us (68%)
  matrix products  76.6 us (12%)
  local copies, waits for them, and re-layouts  60 us (10%)
  starting transfers between devices  21.9 us (4%)
  other arithmetic  14.6 us (2%)
  between operations  13.7 us (2%)
    ppermute x16, waiting for transfers between devices, send(): return lax.ppermute(block, 'sp', route)  282 us
    reduce_scatter x1, waiting for transfers between devices, body(): lax.psum_scatter(partial_value.astype(jnp.bfloat16), 'tp', scatter_dimens...  58.3 us
    reduce_scatter x1, waiting for transfers between devices, body(): ours = lax.psum_scatter(terms[:rows], 'tp', scatter_dimension=0, tiled=True)  40.3 us
    reduce_scatter x1, waiting for transfers between devices, body(): theirs = lax.psum_scatter(second, 'tp', scatter_dimension=0, tiled=True)  37.5 us
    dot_general x7, matrix products, body(): term = jnp.dot(activated, block, preferred_element_type=jnp.float32)  31.4 us
    dot_general x1, matrix products, body(): jnp.dot(normed_whole, up_whole, preferred_element_type=jnp.float32)  24.6 us
    dynamic_update_slice x9, local copies, waits for them, and re-layouts, body(): up_whole = lax.dynamic_update_slice(up_whole, block, (start, 0))  19.9 us
    ppermute x16, starting transfers between devices, send(): return lax.ppermute(block, 'sp', route)  16.9 us
  transfers between devices with their start and end apart: 21, of which 11 were waited for; matrix products, arithmetic and copies ran while one was open for 17% of the time, Pallas kernels for 0%

profile of v1, /device:TPU:0, one launch (start us, length us, event | category | flops | bytes accessed | tf_op | source)
XLA Modules:
  0.0 610.9 jit_solution(1612897437446303681)
XLA Ops:
  8.2 4.9 collective-permute-start
  14.3 2.0 reshape.99
  16.4 2.0 reshape.97
  20.8 1.9 copy.20
  23.4 1.9 copy.16
  25.3 1.7 pad_maximum_fusion
  29.2 5.1 fusion
  34.4 4.5 fusion.1
  40.2 5.0 fusion.29
  45.8 5.4 convolution_convert_fusion
  51.2 58.3 %reduce-scatter.4.cloned.1.call-done = bf16[1024,768]{1,0:T(8,128)(2,1)} async-done(((bf16[1024,3072]{1,0:T(8,128)(2,1)}), bf16[1024,768]{1,0:T(8,128)(2,1)}) %reduce-scatter.4.cloned.1.call-update) | async-done | bytes 1572880 | tf_op jit(solution)/shard_map/reduce_scatter | solution.py:125
  109.5 1.8 add_convert_fusion
  111.7 5.8 psum.7
  119.1 1.7 collective-permute-start.1
  121.2 1.6 collective-permute-start.9
  123.2 50.3 %collective-permute-done.1 = bf16[384,3072]{1,0:T(8,128)(2,1)S(1)} collective-permute-done((bf16[384,3072]{1,0:T(8,128)(2,1)}, bf16[384,3072]{1,0:T(8,128)(2,1)S(1)}, u32[]{:S(2)}, u32[]{:S(2)}) %collective-permute-start.1) | collective-permute-done | bytes 2359328 | tf_op jit(solution)/shard_map/ppermute | solution.py:74
  174.9 1.6 collective-permute-start.3
  177.0 47.1 %collective-permute-done.9 = bf16[3072,384]{1,0:T(8,128)(2,1)S(1)} collective-permute-done((bf16[3072,384]{1,0:T(8,128)(2,1)}, bf16[3072,384]{1,0:T(8,128)(2,1)S(1)}, u32[]{:S(2)}, u32[]{:S(2)}) %collective-permute-start.9) | collective-permute-done | bytes 2359328 | tf_op jit(solution)/shard_map/ppermute | solution.py:74
  224.1 1.6 collective-permute-start.11
  226.1 48.6 %collective-permute-done.3 = bf16[384,3072]{1,0:T(8,128)(2,1)} collective-permute-done((bf16[384,3072]{1,0:T(8,128)(2,1)S(1)}, bf16[384,3072]{1,0:T(8,128)(2,1)}, u32[]{:S(2)}, u32[]{:S(2)}) %collective-permute-start.3) | collective-permute-done | bytes 2359328 | tf_op jit(solution)/shard_map/ppermute | solution.py:74
  274.8 2.1 collective-permute-start.5
  277.3 48.0 %collective-permute-done.11 = bf16[3072,384]{1,0:T(8,128)(2,1)} collective-permute-done((bf16[3072,384]{1,0:T(8,128)(2,1)S(1)}, bf16[3072,384]{1,0:T(8,128)(2,1)}, u32[]{:S(2)}, u32[]{:S(2)}) %collective-permute-start.11) | collective-permute-done | bytes 2359328 | tf_op jit(solution)/shard_map/ppermute | solution.py:74
  325.3 1.6 collective-permute-start.13
  327.3 6.7 %broadcast_in_dim.66 = bf16[3072,3072]{1,0:T(8,128)(2,1)} broadcast(bf16[]{:T(256)} %constant.221.clone.1), dimensions={} | broadcast | bytes 18874370 | tf_op jit(solution)/shard_map/broadcast_in_dim | solution.py:140
  339.7 3.3 constant_dynamic-update-slice_fusion.5
  343.0 32.8 %collective-permute-done.5 = bf16[384,3072]{1,0:T(8,128)(2,1)} collective-permute-done((bf16[384,3072]{1,0:T(8,128)(2,1)}, bf16[384,3072]{1,0:T(8,128)(2,1)}, u32[]{:S(2)}, u32[]{:S(2)}) %collective-permute-start.5) | collective-permute-done | bytes 2359328 | tf_op jit(solution)/shard_map/ppermute | solution.py:74
  377.2 1.7 collective-permute-start.7
  380.7 3.2 constant_dynamic-update-slice_fusion.4
  383.9 42.5 %collective-permute-done.13 = bf16[3072,384]{1,0:T(8,128)(2,1)} collective-permute-done((bf16[3072,384]{1,0:T(8,128)(2,1)}, bf16[3072,384]{1,0:T(8,128)(2,1)}, u32[]{:S(2)}, u32[]{:S(2)}) %collective-permute-start.13) | collective-permute-done | bytes 2359328 | tf_op jit(solution)/shard_map/ppermute | solution.py:74
  426.4 2.4 slice.72
  428.9 1.6 collective-permute-start.15
  430.5 2.4 slice.73
  433.3 3.3 constant_dynamic-update-slice_fusion.3
  436.6 3.2 constant_dynamic-update-slice_fusion.2
  439.8 11.8 %collective-permute-done.7 = bf16[192,3072]{1,0:T(8,128)(2,1)S(1)} collective-permute-done((bf16[192,3072]{1,0:T(8,128)(2,1)S(1)}, bf16[192,3072]{1,0:T(8,128)(2,1)S(1)}, u32[]{:S(2)}, u32[]{:S(2)}) %collective-permute-start.7) | collective-permute-done | bytes 1179680 | tf_op jit(solution)/shard_map/ppermute | solution.py:74
  454.4 24.6 %multiply_convert_fusion = bf16[1024,3072]{1,0:T(8,128)(2,1)S(1)} fusion(bf16[1024,3072]{1,0:T(8,128)(2,1)} %all-gather.2.cloned.1.call-done, bf16[3072,3072]{1,0:T(8,128)(2,1)} %constant_dynamic-update-slice_fusion), kind=kOutput, calls=%fused_computation | convolution fusion | flops 19336790016 | bytes 31457280 | tf_op jit(solution)/shard_map/dot_general | solution.py:147
  480.6 3.5 fusion.16
  484.2 3.5 fusion.18
  487.7 3.5 fusion.20
  491.2 5.2 fusion.22
  496.4 5.2 fusion.24
  501.5 5.2 fusion.26
  506.7 5.4 fusion.28
  512.1 2.3 fusion.53
  514.4 5.1 fusion.33
  519.6 1.7 copy-done.4
  521.9 37.5 %reduce-scatter.8.cloned.1.call-done = bf16[1,1024,384]{2,1,0:T(8,128)(2,1)} async-done(((bf16[4,1024,384]{2,1,0:T(8,128)(2,1)}), bf16[1,1024,384]{2,1,0:T(8,128)(2,1)}) %reduce-scatter.8.cloned.1.call-update) | async-done | bytes 786448 | tf_op jit(solution)/shard_map/reduce_scatter | solution.py:161
  559.4 40.3 %reduce-scatter.6.cloned.1.call-done = bf16[1,1024,384]{2,1,0:T(8,128)(2,1)} async-done(((bf16[4,1024,384]{2,1,0:T(8,128)(2,1)}), bf16[1,1024,384]{2,1,0:T(8,128)(2,1)}) %reduce-scatter.6.cloned.1.call-update) | async-done | bytes 786448 | tf_op jit(solution)/shard_map/reduce_scatter | solution.py:156
  (99 shorter events, 34.6 us)
Async XLA Ops:
  6.5 39.2 %copy-start = (bf16[384,3072]{1,0:T(8,128)(2,1)S(1)}, bf16[384,3072]{1,0:T(8,128)(2,1)}, u32[]{:S(2)}) copy-start(bf16[384,3072]{1,0:T(8,128)(2,1)} %param.13) | copy-start | bytes 7077892
  6.5 18.8 %copy-start.11 = (bf16[1024,128]{1,0:T(8,128)(2,1)S(1)}, bf16[1024,128]{1,0:T(8,128)(2,1)}, u32[]{:S(2)}) copy-start(bf16[1024,128]{1,0:T(8,128)(2,1)} %param.10) | copy-start | bytes 786436
  6.5 103.0 %reduce-scatter.4.cloned.1.call-start = ((), (), s32[]{:S(2)}) async-start(), calls=%async_computation.3 | async-start | bytes 7864320 | tf_op jit(solution)/shard_map/reduce_scatter | solution.py:125
  8.2 17.1 %collective-permute-start = (bf16[128,256]{1,0:T(8,128)(2,1)S(1)}, bf16[128,256]{1,0:T(8,128)(2,1)S(1)}, u32[]{:S(2)}, u32[]{:S(2)}) collective-permute-start(bf16[128,256]{1,0:T(8,128)(2,1)S(1)} %pad_maximum_fusion.2), channel_id=1, source_target_pairs={{0,4},{4,8},{8,12},{12,16},{16,20},{20,24},{24,28},{1,5},{5,9},{9,... | collective-permute-start | bytes 196616 | tf_op jit(solution)/shard_map/ppermute | solution.py:18
  29.2 11.1 %copy-start.12 = (pred[8,128,256]{1,2,0:T(8,128)(4,1)S(1)}, pred[8,128,256]{1,2,0:T(8,128)(4,1)}, u32[]{:S(2)}) copy-start(pred[8,128,256]{1,2,0:T(8,128)(4,1)} %broadcast_and_fusion) | copy-start | bytes 786436
  45.7 5.5 copy-start.13
  51.1 58.4 %copy-start.10 = (bf16[1024,768]{1,0:T(8,128)(2,1)S(1)}, bf16[1024,768]{1,0:T(8,128)(2,1)}, u32[]{:S(2)}) copy-start(bf16[1024,768]{1,0:T(8,128)(2,1)} %param.14) | copy-start | bytes 4718596
  51.2 403.2 %all-gather.2.cloned.1.call-start = ((), (), s32[]{:S(2)}) async-start(), calls=%async_computation.4 | async-start | bytes 7864320 | tf_op jit(solution)/shard_map/all_gather | solution.py:134
  111.3 222.7 %copy-start.2 = (bf16[1024,768]{1,0:T(8,128)(2,1)}, bf16[1024,768]{1,0:T(8,128)(2,1)S(1)}, u32[]{:S(2)}) copy-start(bf16[1024,768]{1,0:T(8,128)(2,1)S(1)} %add_convert_fusion) | copy-start | bytes 4718596
  119.1 440.3 %reduce-scatter.8.cloned.1.call-start = ((), (), s32[]{:S(2)}) async-start(), calls=%async_computation.6 | async-start | bytes 3932160 | tf_op jit(solution)/shard_map/reduce_scatter | solution.py:161
  119.1 54.4 %collective-permute-start.1 = (bf16[384,3072]{1,0:T(8,128)(2,1)}, bf16[384,3072]{1,0:T(8,128)(2,1)S(1)}, u32[]{:S(2)}, u32[]{:S(2)}) collective-permute-start(bf16[384,3072]{1,0:T(8,128)(2,1)} %param.16), channel_id=1, source_target_pairs={{0,8},{8,16},{16,24},{24,28},{28,20},{20,12},{12,4},{4,0},{1,9},{9... | collective-permute-start | bytes 7077896 | tf_op jit(solution)/shard_map/ppermute | solution.py:74
  120.8 55.7 %collective-permute-start.2 = (bf16[384,3072]{1,0:T(8,128)(2,1)}, bf16[384,3072]{1,0:T(8,128)(2,1)S(1)}, u32[]{:S(2)}, u32[]{:S(2)}) collective-permute-start(bf16[384,3072]{1,0:T(8,128)(2,1)} %param.16), channel_id=1, source_target_pairs={{8,0},{16,8},{24,16},{28,24},{20,28},{12,20},{4,12},{0,4},{9,1},{1... | collective-permute-start | bytes 7077896 | tf_op jit(solution)/shard_map/ppermute | solution.py:74
  121.2 102.9 %collective-permute-start.9 = (bf16[3072,384]{1,0:T(8,128)(2,1)}, bf16[3072,384]{1,0:T(8,128)(2,1)S(1)}, u32[]{:S(2)}, u32[]{:S(2)}) collective-permute-start(bf16[3072,384]{1,0:T(8,128)(2,1)} %param.17), channel_id=1, source_target_pairs={{0,8},{8,16},{16,24},{24,28},{28,20},{20,12},{12,4},{4,0},{1,9},{9... | collective-permute-start | bytes 7077896 | tf_op jit(solution)/shard_map/ppermute | solution.py:74
  122.9 102.9 %collective-permute-start.10 = (bf16[3072,384]{1,0:T(8,128)(2,1)}, bf16[3072,384]{1,0:T(8,128)(2,1)S(1)}, u32[]{:S(2)}, u32[]{:S(2)}) collective-permute-start(bf16[3072,384]{1,0:T(8,128)(2,1)} %param.17), channel_id=1, source_target_pairs={{8,0},{16,8},{24,16},{28,24},{20,28},{12,20},{4,12},{0,4},{9,1},{1... | collective-permute-start | bytes 7077896 | tf_op jit(solution)/shard_map/ppermute | solution.py:74
  173.5 1.4 copy-start.6
  174.9 99.8 %collective-permute-start.3 = (bf16[384,3072]{1,0:T(8,128)(2,1)S(1)}, bf16[384,3072]{1,0:T(8,128)(2,1)}, u32[]{:S(2)}, u32[]{:S(2)}) collective-permute-start(bf16[384,3072]{1,0:T(8,128)(2,1)S(1)} %collective-permute-done.1), channel_id=1, source_target_pairs={{0,8},{8,16},{16,24},{24,28},{28,20},{20,12},{12,4},{4,0},{1,9},{9... | collective-permute-start | bytes 7077896 | tf_op jit(solution)/shard_map/ppermute | solution.py:74
  176.6 98.2 %copy-start.8 = (bf16[384,3072]{1,0:T(8,128)(2,1)}, bf16[384,3072]{1,0:T(8,128)(2,1)S(1)}, u32[]{:S(2)}) copy-start(bf16[384,3072]{1,0:T(8,128)(2,1)S(1)} %collective-permute-done.2) | copy-start | bytes 7077892
  176.6 100.3 %collective-permute-start.4 = (bf16[384,3072]{1,0:T(8,128)(2,1)S(1)}, bf16[384,3072]{1,0:T(8,128)(2,1)}, u32[]{:S(2)}, u32[]{:S(2)}) collective-permute-start(bf16[384,3072]{1,0:T(8,128)(2,1)S(1)} %collective-permute-done.2), channel_id=1, source_target_pairs={{8,0},{16,8},{24,16},{28,24},{20,28},{12,20},{4,12},{0,4},{9,1},{1... | collective-permute-start | bytes 7077896 | tf_op jit(solution)/shard_map/ppermute | solution.py:74
  224.1 52.8 %copy-start.15 = (bf16[3072,384]{1,0:T(8,128)(2,1)}, bf16[3072,384]{1,0:T(8,128)(2,1)S(1)}, u32[]{:S(2)}) copy-start(bf16[3072,384]{1,0:T(8,128)(2,1)S(1)} %collective-permute-done.9) | copy-start | bytes 7077892
  224.1 101.2 %collective-permute-start.11 = (bf16[3072,384]{1,0:T(8,128)(2,1)S(1)}, bf16[3072,384]{1,0:T(8,128)(2,1)}, u32[]{:S(2)}, u32[]{:S(2)}) collective-permute-start(bf16[3072,384]{1,0:T(8,128)(2,1)S(1)} %collective-permute-done.9), channel_id=1, source_target_pairs={{0,8},{8,16},{16,24},{24,28},{28,20},{20,12},{12,4},{4,0},{1,9},{9... | collective-permute-start | bytes 7077896 | tf_op jit(solution)/shard_map/ppermute | solution.py:74
  225.7 99.6 %copy-start.17 = (bf16[3072,384]{1,0:T(8,128)(2,1)}, bf16[3072,384]{1,0:T(8,128)(2,1)S(1)}, u32[]{:S(2)}) copy-start(bf16[3072,384]{1,0:T(8,128)(2,1)S(1)} %collective-permute-done.10) | copy-start | bytes 7077892
  225.7 101.2 %collective-permute-start.12 = (bf16[3072,384]{1,0:T(8,128)(2,1)S(1)}, bf16[3072,384]{1,0:T(8,128)(2,1)}, u32[]{:S(2)}, u32[]{:S(2)}) collective-permute-start(bf16[3072,384]{1,0:T(8,128)(2,1)S(1)} %collective-permute-done.10), channel_id=1, source_target_pairs={{8,0},{16,8},{24,16},{28,24},{20,28},{12,20},{4,12},{0,4},{9,1},{1... | collective-permute-start | bytes 7077896 | tf_op jit(solution)/shard_map/ppermute | solution.py:74
  274.8 101.1 %collective-permute-start.5 = (bf16[384,3072]{1,0:T(8,128)(2,1)}, bf16[384,3072]{1,0:T(8,128)(2,1)}, u32[]{:S(2)}, u32[]{:S(2)}) collective-permute-start(bf16[384,3072]{1,0:T(8,128)(2,1)} %collective-permute-done.3), channel_id=1, source_target_pairs={{0,8},{8,16},{16,24},{24,28},{28,20},{20,12},{12,4},{4,0},{1,9},{9... | collective-permute-start | bytes 7077896 | tf_op jit(solution)/shard_map/ppermute | solution.py:74
  276.9 102.0 %collective-permute-start.6 = (bf16[384,3072]{1,0:T(8,128)(2,1)}, bf16[384,3072]{1,0:T(8,128)(2,1)}, u32[]{:S(2)}, u32[]{:S(2)}) collective-permute-start(bf16[384,3072]{1,0:T(8,128)(2,1)} %collective-permute-done.4), channel_id=1, source_target_pairs={{8,0},{16,8},{24,16},{28,24},{20,28},{12,20},{4,12},{0,4},{9,1},{1... | collective-permute-start | bytes 7077896 | tf_op jit(solution)/shard_map/ppermute | solution.py:74
  325.3 101.1 %collective-permute-start.13 = (bf16[3072,384]{1,0:T(8,128)(2,1)}, bf16[3072,384]{1,0:T(8,128)(2,1)}, u32[]{:S(2)}, u32[]{:S(2)}) collective-permute-start(bf16[3072,384]{1,0:T(8,128)(2,1)} %collective-permute-done.11), channel_id=1, source_target_pairs={{0,8},{8,16},{16,24},{24,28},{28,20},{20,12},{12,4},{4,0},{1,9},{9... | collective-permute-start | bytes 7077896 | tf_op jit(solution)/shard_map/ppermute | solution.py:74
  327.0 103.6 %collective-permute-start.14 = (bf16[3072,384]{1,0:T(8,128)(2,1)}, bf16[3072,384]{1,0:T(8,128)(2,1)}, u32[]{:S(2)}, u32[]{:S(2)}) collective-permute-start(bf16[3072,384]{1,0:T(8,128)(2,1)} %collective-permute-done.12), channel_id=1, source_target_pairs={{8,0},{16,8},{24,16},{28,24},{20,28},{12,20},{4,12},{0,4},{9,1},{1... | collective-permute-start | bytes 7077896 | tf_op jit(solution)/shard_map/ppermute | solution.py:74
  327.3 6.7 %copy-start.5 = (bf16[384,3072]{1,0:T(8,128)(2,1)S(1)}, bf16[384,3072]{1,0:T(8,128)(2,1)}, u32[]{:S(2)}) copy-start(bf16[384,3072]{1,0:T(8,128)(2,1)} %param.16) | copy-start | bytes 7077892
  334.0 2.5 copy-start.7
  334.0 4.1 copy-start.9
  377.2 74.4 %collective-permute-start.7 = (bf16[192,3072]{1,0:T(8,128)(2,1)S(1)}, bf16[192,3072]{1,0:T(8,128)(2,1)S(1)}, u32[]{:S(2)}, u32[]{:S(2)}) collective-permute-start(bf16[192,3072]{1,0:T(8,128)(2,1)S(1)} %slice.68), channel_id=1, source_target_pairs={{0,8},{8,16},{16,24},{24,28},{28,20},{20,12},{12,4},{4,0},{1,9},{9... | collective-permute-start | bytes 3538952 | tf_op jit(solution)/shard_map/ppermute | solution.py:74
  380.3 73.0 %collective-permute-start.8 = (bf16[192,3072]{1,0:T(8,128)(2,1)S(1)}, bf16[192,3072]{1,0:T(8,128)(2,1)S(1)}, u32[]{:S(2)}, u32[]{:S(2)}) collective-permute-start(bf16[192,3072]{1,0:T(8,128)(2,1)S(1)} %slice.69), channel_id=1, source_target_pairs={{8,0},{16,8},{24,16},{28,24},{20,28},{12,20},{4,12},{0,4},{9,1},{1... | collective-permute-start | bytes 3538952 | tf_op jit(solution)/shard_map/ppermute | solution.py:74
  428.9 85.6 %collective-permute-start.15 = (bf16[1536,384]{1,0:T(8,128)(2,1)}, bf16[1536,384]{1,0:T(8,128)(2,1)}, u32[]{:S(2)}, u32[]{:S(2)}) collective-permute-start(bf16[1536,384]{1,0:T(8,128)(2,1)} %slice.72), channel_id=1, source_target_pairs={{0,8},{8,16},{16,24},{24,28},{28,20},{20,12},{12,4},{4,0},{1,9},{9... | collective-permute-start | bytes 3538952 | tf_op jit(solution)/shard_map/ppermute | solution.py:74
  433.0 81.5 %collective-permute-start.16 = (bf16[1536,384]{1,0:T(8,128)(2,1)}, bf16[1536,384]{1,0:T(8,128)(2,1)}, u32[]{:S(2)}, u32[]{:S(2)}) collective-permute-start(bf16[1536,384]{1,0:T(8,128)(2,1)} %slice.73), channel_id=1, source_target_pairs={{8,0},{16,8},{24,16},{28,24},{20,28},{12,20},{4,12},{0,4},{9,1},{1... | collective-permute-start | bytes 3538952 | tf_op jit(solution)/shard_map/ppermute | solution.py:74
  479.0 1.7 copy-start.14
  480.6 3.5 copy-start.16
  484.2 3.5 copy-start.18
  519.6 1.7 copy-start.4
  521.3 78.4 %reduce-scatter.6.cloned.1.call-start = ((), (), s32[]{:S(2)}) async-start(), calls=%async_computation.5 | async-start | bytes 3932160 | tf_op jit(solution)/shard_map/reduce_scatter | solution.py:156
  601.2 1.4 copy-start.3
  601.2 2.9 copy-start.1
Sparse Core Ops, SparseCore 0:
  51.3 58.1 reduce-scatter.3
  119.2 46.9 all-gather.1
  521.4 37.9 reduce-scatter.7
  561.8 37.8 reduce-scatter.5
